TPU v7x, 32 devices: a whole 2x2x4 slice. The times are simulated.
32 devices in a mesh: ep: 8 (over z, x), tp: 4 (over y, core).
Axes of the slice: x: 2, y: 2, z: 4, core: 2. Of those that a mesh axis runs over, the one named last changes fastest.
Arguments:
- query_rows: bfloat16 [2048, 1024], P('ep', 'tp'), may hold values from -8 to 8
- key_rows: bfloat16 [2048, 256], P('ep', 'tp'), may hold values from -8 to 8
- value_rows: bfloat16 [2048, 256], P('ep', 'tp'), may hold values from -16 to 16
- query_gain: float32 [64], replicated, may hold values from 0.5 to 7.5
- key_gain: float32 [64], replicated, may hold values from 0.5 to 7.5
- moe_tokens: bfloat16 [4096, 2048], P(('ep', 'tp')), may hold values from -6 to 6
- norm_gain: float32 [2048], replicated, may hold values from 0.1 to 1.9
- routes: int32 [4096, 2], P('ep'), may hold values from 0 to 7, all different within a row; in each aligned block of 128 rows (0 to 127, 128 to 255, ...) at most 64 rows name the same one
- route_weights: float32 [4096, 2], P('ep'), may hold values from 0.1 to 1
- expert_gate: bfloat16 [8, 2048, 1024], P('ep', None, 'tp'), may hold values from -0.125 to 0.125
- expert_up: bfloat16 [8, 2048, 1024], P('ep', None, 'tp'), may hold values from -0.125 to 0.125
- expert_down: bfloat16 [8, 1024, 2048], P('ep', 'tp'), may hold values from -0.1875 to 0.1875
- shared_gate: bfloat16 [2048, 1024], P(None, 'tp'), may hold values from -0.125 to 0.125
- shared_up: bfloat16 [2048, 1024], P(None, 'tp'), may hold values from -0.125 to 0.125
- shared_down: bfloat16 [1024, 2048], P('tp'), may hold values from -0.1875 to 0.1875
Outputs:
- attn_out: bfloat16 [2048, 1024], P('ep', 'tp')
- moe_out: bfloat16 [4096, 2048], P(('ep', 'tp'))
Inputs may be any that keep to these rules, and one draw needn't show every extreme that they name: `routes`: each row names 2 different experts. Within each aligned block of 128 rows no expert is named more than 64 times, and in every draw some expert is named exactly 64 times in some block.
All inputs are finite; a program needn't handle non-finite values.
Results may differ from a plain program's by a relative error of at most 0.012.
The roundings to bfloat16 on the way count: a program that leaves them out, or rounds other values in their place, can miss the bound.
Values may be sent and summed in bfloat16 or wider, within the bound.
A program may use at most 192 MiB of HBM per device.

v0:
```python
import jax
import jax.numpy as jnp
from jax import lax
from jax.sharding import PartitionSpec as P

GRID_W = 64
epsilon = 1e-06
rotary_base = 10000.0
routed_scale = 2.5


def rotate_heads(heads_in, gain_row, positions):
    values32 = heads_in.astype(jnp.float32)
    scaled = (
        values32
        * lax.rsqrt(jnp.mean(values32 * values32, axis=-1, keepdims=True) + epsilon)
        * gain_row
    )
    pair_count = scaled.shape[-1] // 4
    inv_freq = rotary_base ** (-jnp.arange(pair_count, dtype=jnp.float32) / pair_count)
    grid_row = (positions // GRID_W).astype(jnp.float32)
    grid_col = (positions % GRID_W).astype(jnp.float32)
    angles = jnp.concatenate([grid_row[:, None] * inv_freq, grid_col[:, None] * inv_freq], axis=-1)[
        :, None, :
    ]
    cosine = jnp.cos(angles)
    sine_part = jnp.sin(angles)
    first_half = scaled[..., 0::2]
    second_half = scaled[..., 1::2]
    turned = jnp.stack(
        [
            first_half * cosine - second_half * sine_part,
            first_half * sine_part + second_half * cosine,
        ],
        axis=-1,
    )
    return turned.reshape(scaled.shape).astype(jnp.bfloat16)


def span_length(row_count):
    length = min(row_count, 2048)
    while row_count % length:
        length -= 1
    return length


def attend(query_rows, key_rows, value_rows, query_gain, key_gain):
    row_count = query_rows.shape[0]
    head_size = query_gain.shape[0]
    q_heads = query_rows.shape[1] // head_size
    kv_heads = key_rows.shape[1] // head_size
    group = q_heads // kv_heads
    scale = head_size ** (-0.5)
    positions = lax.axis_index("ep") * row_count + jnp.arange(row_count, dtype=jnp.int32)
    q_rot = rotate_heads(query_rows.reshape(row_count, q_heads, head_size), query_gain, positions)
    k_rot = rotate_heads(key_rows.reshape(row_count, kv_heads, head_size), key_gain, positions)
    key_value = jnp.stack([k_rot, value_rows.reshape(row_count, kv_heads, head_size)], axis=2)
    key_value = key_value.reshape(row_count, kv_heads * 2 * head_size)
    q_grouped = q_rot.reshape(row_count, kv_heads, group, head_size).transpose(1, 2, 0, 3)
    q_grouped = q_grouped.reshape(kv_heads, group * row_count, head_size)
    query_count = group * row_count
    initial = (
        jnp.full((kv_heads, query_count), -jnp.inf, jnp.float32),
        jnp.zeros((kv_heads, query_count), jnp.float32),
        jnp.zeros((kv_heads, query_count, head_size), jnp.float32),
    )

    def one_span(carried, span_rows):
        run_max, run_sum, mixed = carried
        keys_span = span_rows[:, :, 0, :]
        values_span = span_rows[:, :, 1, :]
        scores = (
            jnp.einsum("hrd,shd->hrs", q_grouped, keys_span, preferred_element_type=jnp.float32)
            * scale
        )
        new_max = jnp.maximum(run_max, jnp.max(scores, axis=-1))
        factor = jnp.exp(run_max - new_max)
        weights = jnp.exp(scores - new_max[..., None])
        run_sum = run_sum * factor + jnp.sum(weights, axis=-1)
        added = jnp.einsum(
            "hrs,shd->hrd",
            weights.astype(jnp.bfloat16),
            values_span,
            preferred_element_type=jnp.float32,
        )
        mixed = mixed * factor[..., None] + added
        return ((new_max, run_sum, mixed), None)

    carried = initial
    piece_rows = lax.all_gather(key_value, "ep", axis=0, tiled=True)
    piece_count = piece_rows.shape[0]
    length = span_length(piece_count)
    spans = piece_rows.reshape(piece_count // length, length, kv_heads, 2, head_size)
    carried, unused = lax.scan(one_span, carried, spans)
    run_max, run_sum, mixed = carried
    result = (mixed / run_sum[..., None]).astype(jnp.bfloat16)
    result = result.reshape(kv_heads, group, row_count, head_size).transpose(2, 0, 1, 3)
    return result.reshape(row_count, q_heads * head_size)


def slot_ranks(route_rows, tok_rows, experts):
    top_count = route_rows.shape[1]
    blocks = route_rows.shape[0] // tok_rows
    chosen = route_rows.reshape(blocks, tok_rows * top_count)
    one_hot = (chosen[:, :, None] == jnp.arange(experts, dtype=jnp.int32)[None, None, :]).astype(
        jnp.int32
    )
    ranks = jnp.sum((jnp.cumsum(one_hot, axis=1) - one_hot) * one_hot, axis=2)
    return (chosen, ranks)


def build_send(source, chosen, ranks, tok_rows, top_count, capacity, experts):
    blocks = chosen.shape[0]
    model_width = source.shape[1]
    block_ids = jnp.arange(blocks, dtype=jnp.int32)[:, None]
    dest = (chosen * blocks + block_ids) * capacity + ranks
    rows_from = (
        block_ids * tok_rows
        + jnp.arange(tok_rows * top_count, dtype=jnp.int32)[None, :] // top_count
    )
    slot_rows = jnp.full((experts * blocks * capacity,), blocks * tok_rows, jnp.int32)
    slot_rows = slot_rows.at[dest.reshape(-1)].set(rows_from.reshape(-1))
    padded = jnp.concatenate([source, jnp.zeros((1, model_width), source.dtype)], axis=0)
    return padded[slot_rows].reshape(experts, blocks * capacity, model_width)


def expert_products(arrived, w_gate, w_up, w_down):
    gate_proj = jnp.einsum("lrd,ldf->lrf", arrived, w_gate, preferred_element_type=jnp.float32)
    up_proj = jnp.einsum("lrd,ldf->lrf", arrived, w_up, preferred_element_type=jnp.float32)
    hidden = (jax.nn.silu(gate_proj) * up_proj).astype(jnp.bfloat16)
    return jnp.einsum("lrf,lfd->lrd", hidden, w_down, preferred_element_type=jnp.float32)


def shared_products(rows_in, w_gate, w_up, w_down):
    gate_proj = jnp.dot(rows_in, w_gate, preferred_element_type=jnp.float32)
    up_proj = jnp.dot(rows_in, w_up, preferred_element_type=jnp.float32)
    hidden = (jax.nn.silu(gate_proj) * up_proj).astype(jnp.bfloat16)
    return jnp.dot(hidden, w_down, preferred_element_type=jnp.float32)


def experts_half(
    moe_tokens,
    norm_gain,
    routes,
    route_weights,
    expert_gate,
    expert_up,
    expert_down,
    shared_gate,
    shared_up,
    shared_down,
):
    tok_rows, model_width = moe_tokens.shape
    top_count = routes.shape[1]
    tp_size = lax.axis_size("tp")
    ep_size = lax.axis_size("ep")
    local_experts = expert_gate.shape[0]
    experts = local_experts * ep_size
    capacity = 2 * tok_rows * top_count // experts
    lane = lax.axis_index("tp")
    values32 = moe_tokens.astype(jnp.float32)
    normed = (
        values32
        * lax.rsqrt(jnp.mean(values32 * values32, axis=-1, keepdims=True) + epsilon)
        * norm_gain
    ).astype(jnp.bfloat16)
    gates = route_weights / jnp.sum(route_weights, axis=-1, keepdims=True) * routed_scale
    own_gates = lax.dynamic_slice_in_dim(gates, lane * tok_rows, tok_rows, 0)
    own_routes = lax.dynamic_slice_in_dim(routes, lane * tok_rows, tok_rows, 0)
    chosen, ranks = slot_ranks(own_routes, tok_rows, experts)
    send = build_send(normed, chosen, ranks, tok_rows, top_count, capacity, experts)
    landed = lax.all_to_all(send, "ep", split_axis=0, concat_axis=1, tiled=True)
    arrived, group_rows = (
        lax.all_gather(
            landed.reshape(local_experts, ep_size, 1, capacity, model_width),
            "tp",
            axis=2,
            tiled=True,
        ),
        lax.all_gather(normed.reshape(1, 1, 1, tok_rows, model_width), "tp", axis=2, tiled=True),
    )
    own_chosen = chosen[0]
    own_ranks = ranks[0]
    arrived = arrived.reshape(local_experts, ep_size * tp_size * capacity, model_width)
    routed_part = expert_products(arrived, expert_gate, expert_up, expert_down)
    shared_part = shared_products(
        group_rows.reshape(tp_size * tok_rows, model_width), shared_gate, shared_up, shared_down
    )
    routed_sum, shared_sum = (
        lax.psum_scatter(
            routed_part.reshape(local_experts, ep_size, tp_size, capacity, model_width).astype(
                jnp.bfloat16
            ),
            "tp",
            scatter_dimension=2,
            tiled=True,
        ).astype(jnp.float32),
        lax.psum_scatter(
            shared_part.reshape(1, 1, tp_size, tok_rows, model_width).astype(jnp.bfloat16),
            "tp",
            scatter_dimension=2,
            tiled=True,
        ).astype(jnp.float32),
    )
    outgoing = routed_sum.astype(jnp.bfloat16).reshape(
        local_experts, ep_size * capacity, model_width
    )
    returned = lax.all_to_all(outgoing, "ep", split_axis=1, concat_axis=0, tiled=True)
    flat_rows = returned.reshape(experts * capacity, model_width)
    picked = flat_rows[own_chosen * capacity + own_ranks].reshape(tok_rows, top_count, model_width)
    routed_total = jnp.sum(own_gates[:, :, None] * picked.astype(jnp.float32), axis=1)
    return (routed_total + shared_sum.reshape(tok_rows, model_width)).astype(jnp.bfloat16)


def body(
    query_rows,
    key_rows,
    value_rows,
    query_gain,
    key_gain,
    moe_tokens,
    norm_gain,
    routes,
    route_weights,
    expert_gate,
    expert_up,
    expert_down,
    shared_gate,
    shared_up,
    shared_down,
):
    attn_out = attend(query_rows, key_rows, value_rows, query_gain, key_gain)
    moe_out = experts_half(
        moe_tokens,
        norm_gain,
        routes,
        route_weights,
        expert_gate,
        expert_up,
        expert_down,
        shared_gate,
        shared_up,
        shared_down,
    )
    return (attn_out, moe_out)


def solution(mesh):
    return jax.shard_map(
        body,
        mesh=mesh,
        in_specs=(
            P("ep", "tp"),
            P("ep", "tp"),
            P("ep", "tp"),
            P(),
            P(),
            P(("ep", "tp"), None),
            P(),
            P("ep", None),
            P("ep", None),
            P("ep", None, "tp"),
            P("ep", None, "tp"),
            P("ep", "tp", None),
            P(None, "tp"),
            P(None, "tp"),
            P("tp", None),
        ),
        out_specs=(P("ep", "tp"), P(("ep", "tp"), None)),
        check_vma=False,
    )
```

profile of v0, /device:TPU:0, one launch (start us, length us, event | category | flops | bytes accessed | tf_op | source)
XLA Modules:
  0.0 441.3 jit_solution(13202950709804458420)
XLA Ops:
  7.2 0.8 broadcast_multiply_fusion.2
  9.5 1.4 scatter_custom_fusion
  10.9 1.2 fusion.15
  12.2 1.2 fusion.17
  13.5 3.3 gather_fusion
  16.8 55.6 %all_to_all.8 = bf16[8,64,2048]{2,1,0:T(8,128)(2,1)} all-to-all(bf16[8,64,2048]{2,1,0:T(8,128)(2,1)} %bitcast.110), channel_id=1, replica_groups=mesh['ep'=8,'tp'=4] {'ep'}, dimensions={0} | all-to-all | bytes 4194304 | tf_op jit(solution)/shard_map/all_to_all | solution.py:172
  72.5 0.7 all-gather.7.cloned.1.call-update
  73.3 56.7 %all-gather.5.cloned.1.call-done = bf16[8,256,2048]{2,1,0:T(8,128)(2,1)} async-done(((bf16[8,64,2048]{2,1,0:T(8,128)(2,1)}), bf16[8,256,2048]{2,1,0:T(8,128)(2,1)}) %all-gather.5.cloned.1.call-update) | async-done | bytes 8388624 | tf_op jit(solution)/shard_map/all_gather | solution.py:174
  129.9 5.9 %fusion.21 = f32[2048,256]{1,0:T(8,128)S(1)} fusion(bf16[2048,2048]{1,0:T(8,128)(2,1)} %bitcast.125, bf16[1,2048,256]{2,1,0:T(8,128)(2,1)S(1)} %copy-done.11), kind=kOutput, calls=%fused_computation.28 | convolution fusion | flops 2147483648 | bytes 11534336 | tf_op jit(solution)/shard_map/lrd,ldf->lrf/dot_general | solution.py:128
  135.9 2.6 fusion.4
  138.6 5.6 %convert_bitcast_fusion = bf16[1,8,4,64,2048]{4,3,2,1,0:T(8,128)(2,1)} fusion(bf16[8,4,64,256]{3,2,1,0:T(8,128)(2,1)S(1)} %bitcast.113, bf16[1,256,2048]{2,1,0:T(8,128)(2,1)S(1)} %copy-done), kind=kOutput, calls=%fused_computation.3 | convolution fusion | flops 2151677952 | bytes 10485760 | tf_op jit(solution)/shard_map/lrf,lfd->lrd/dot_general | solution.py:131
  144.4 0.6 copy-done.4
  146.3 8.4 %all-gather.7.cloned.1.call-done = bf16[512,2048]{1,0:T(8,128)(2,1)} async-done(((bf16[128,2048]{1,0:T(8,128)(2,1)}), bf16[512,2048]{1,0:T(8,128)(2,1)}) %all-gather.7.cloned.1.call-update) | async-done | bytes 2097168 | tf_op jit(solution)/shard_map/all_gather | solution.py:180
  154.6 3.5 fusion.56
  158.2 5.4 %convolution_convert_fusion = bf16[512,2048]{1,0:T(8,128)(2,1)} fusion(bf16[256,2048]{1,0:T(8,128)(2,1)} %param.29, bf16[512,2048]{1,0:T(8,128)(2,1)S(1)} %copy-done.10, bf16[2048,256]{1,0:T(8,128)(2,1)} %param.28, f32[512,256]{1,0:T(8,128)} %fusion.56), kind=kOutput, calls=%fused_computation.9 | convolution fusion | flops 1075576832 | bytes 6815744 | tf_op jit(solution)/shard_map/dot_general | solution.py:138
  163.5 146.5 %all-reduce.4.cloned.1.call-done = bf16[1,8,4,64,2048]{4,3,2,1,0:T(8,128)(2,1)} async-done(((bf16[1,8,4,64,2048]{4,3,2,1,0:T(8,128)(2,1)}), bf16[1,8,4,64,2048]{4,3,2,1,0:T(8,128)(2,1)}) %all-reduce.4.cloned.1.call-update) | async-done | bytes 8388624
  310.0 2.5 constant_dynamic-slice_fusion
  312.5 5.2 %copy.56 = bf16[1,512,2048]{2,0,1:T(2,128)(2,1)} copy(bf16[1,512,2048]{2,1,0:T(8,128)(2,1)S(1)} %bitcast.111) | data formatting | bytes 4194304 | tf_op jit(solution)/shard_map/reshape | solution.py:205
  318.2 13.2 %reduce.9 = bf16[512,2048]{1,0:T(8,128)(2,1)S(1)} reduce(bf16[512,1,2048]{2,1,0:T(2,128)(2,1)} %bitcast.108, bf16[]{:T(256)} %broadcast.377), dimensions={1}, to_apply=%bitcast.106.reduce_sub_computation | reduce | bytes 4194306
  331.4 3.8 reshape.653
  335.2 5.6 %all-to-all-start.1 = ((bf16[8,2,65536]{2,1,0:T(2,128)(2,1)}), bf16[8,2,65536]{2,1,0:T(2,128)(2,1)S(1)}, u32[]{:S(2)}, u32[]{:S(2)}) async-start(bf16[8,2,65536]{2,1,0:T(2,128)(2,1)} %reshape.653), calls=%async_computation.1 | async-start | bytes 4194304 | tf_op jit(solution)/shard_map/all_to_all | solution.py:208
  341.7 68.2 %all_gather.9 = bf16[2048,128]{0,1:T(8,128)(2,1)S(1)} all-gather(bf16[256,128]{0,1:T(8,128)(2,1)S(1)} %bitcast.119), channel_id=1, replica_groups=mesh['ep'=8,'tp'=4] {'ep'}, dimensions={0}, use_global_device_ids=true | all-gather | bytes 589824 | tf_op jit(solution)/shard_map/all_gather | solution.py:90
  409.9 1.4 multiply_reduce_fusion
  411.3 1.9 fusion
  413.2 1.7 fusion.12
  415.0 0.8 copy.47
  415.8 4.4 reshape.654
  420.2 3.5 copy.55
  423.7 2.3 gather_fusion.1
  426.0 2.5 reshape.614
  428.5 4.1 multiply_reduce_fusion.1
  432.5 2.3 fusion.18
  (86 shorter events, 4.6 us)
Async XLA Ops:
  7.2 131.4 %copy-start = (bf16[1,256,2048]{2,1,0:T(8,128)(2,1)S(1)}, bf16[1,256,2048]{2,1,0:T(8,128)(2,1)}, u32[]{:S(2)}) copy-start(bf16[1,256,2048]{2,1,0:T(8,128)(2,1)} %param.26) | copy-start | bytes 3145732
  7.2 122.7 %all-gather.5.cloned.1.call-start = ((), (), s32[]{:S(2)}) async-start(), calls=%async_computation.4 | async-start | bytes 10485760 | tf_op jit(solution)/shard_map/all_gather | solution.py:174
  13.4 3.4 copy-start.2
  72.4 57.5 %copy-start.11 = (bf16[1,2048,256]{2,1,0:T(8,128)(2,1)S(1)}, bf16[1,2048,256]{2,1,0:T(8,128)(2,1)}, u32[]{:S(2)}) copy-start(bf16[1,2048,256]{2,1,0:T(8,128)(2,1)} %param.24) | copy-start | bytes 3145732
  72.5 82.2 %all-gather.7.cloned.1.call-start = ((), (), s32[]{:S(2)}) async-start(), calls=%async_computation.5 | async-start | bytes 2621440 | tf_op jit(solution)/shard_map/all_gather | solution.py:180
  73.2 236.8 %all-reduce.4.cloned.1.call-start = ((), (), s32[]{:S(2)}) async-start(), calls=%async_computation.6 | async-start | bytes 16777216
  129.9 5.9 %copy-start.9 = (bf16[8,256,2048]{2,1,0:T(8,128)(2,1)S(1)}, bf16[8,256,2048]{2,1,0:T(8,128)(2,1)}, u32[]{:S(2)}) copy-start(bf16[8,256,2048]{2,1,0:T(8,128)(2,1)} %all-gather.5.cloned.1.call-done) | copy-start | bytes 25165828
  129.9 6.0 %copy-start.12 = (bf16[1,2048,256]{2,1,0:T(8,128)(2,1)S(1)}, bf16[1,2048,256]{2,1,0:T(8,128)(2,1)}, u32[]{:S(2)}) copy-start(bf16[1,2048,256]{2,1,0:T(8,128)(2,1)} %param.25) | copy-start | bytes 3145732
  144.1 0.9 copy-start.4
  144.1 1.1 copy-start.7
  144.1 1.3 copy-start.3
  144.1 1.3 copy-start.8
  144.1 1.4 copy-start.6
  144.1 1.5 copy-start.13
  144.2 288.4 %reduce-scatter.5.cloned.1.call-start = ((), (), s32[]{:S(2)}) async-start(), calls=%async_computation.3 | async-start | bytes 2621440 | tf_op jit(solution)/shard_map/reduce_scatter | solution.py:198
  154.6 3.5 copy-start.10
  335.2 6.4 %copy-start.5 = (bf16[256,64]{0,1:T(8,128)(2,1)S(1)}, bf16[256,64]{0,1:T(8,128)(2,1)}, u32[]{:S(2)}) copy-start(bf16[256,64]{0,1:T(8,128)(2,1)} %param.17) | copy-start | bytes 98308
  335.2 80.5 %all-to-all-start.1 = ((bf16[8,2,65536]{2,1,0:T(2,128)(2,1)}), bf16[8,2,65536]{2,1,0:T(2,128)(2,1)S(1)}, u32[]{:S(2)}, u32[]{:S(2)}) async-start(bf16[8,2,65536]{2,1,0:T(2,128)(2,1)} %reshape.653), calls=%async_computation.1 | async-start | bytes 4194304 | tf_op jit(solution)/shard_map/all_to_all | solution.py:208
  426.0 8.8 %copy-start.1 = (bf16[1,256,2048]{2,1,0:T(8,128)(2,1)S(1)}, bf16[1,256,2048]{2,1,0:T(8,128)(2,1)}, u32[]{:S(2)}) copy-start(bf16[1,256,2048]{2,1,0:T(8,128)(2,1)} %param.26) | copy-start | bytes 3145732
Sparse Core Ops, SparseCore 0:
  72.6 57.2 all-gather.4
  132.0 22.5 all-gather.6
  157.1 152.8 all-reduce.3
  312.4 31.3 reduce-scatter.4
where the time goes:
time: 442 us; the launch traced here: 441 us
  waiting for transfers between devices  212 us (48%)
  blocking collectives  124 us (28%)
  local copies, waits for them, and re-layouts  33 us (7%)
  other arithmetic  26.2 us (6%)
  matrix products  26 us (6%)
  between operations  14.2 us (3%)
  starting transfers between devices  5.97 us (1%)
    unnamed x5, waiting for transfers between devices  147 us
    all_gather x1, blocking collectives, attend(): piece_rows = lax.all_gather(key_value, 'ep', axis=0, tiled=True)  68.2 us
    all_gather x1, waiting for transfers between devices, experts_half(): lax.all_gather(landed.reshape(local_experts, ep_size, 1, capacity, model_...  56.7 us
    all_to_all x1, blocking collectives, experts_half(): landed = lax.all_to_all(send, 'ep', split_axis=0, concat_axis=1, tiled=True)  55.6 us
    unnamed x37, local copies, waits for them, and re-layouts  16.9 us
    unnamed x1, other arithmetic  13.2 us
  transfers between devices with their start and end apart: 5, of which 3 were waited for; matrix products, arithmetic and copies ran while one was open for 16% of the time, Pallas kernels for 0%

commit v1 on v0

--- a/solution.py
+++ b/solution.py
@@ -87,7 +87,12 @@
         return ((new_max, run_sum, mixed), None)
 
     carried = initial
-    piece_rows = lax.all_gather(key_value, "ep", axis=0, tiled=True)
+    ring = [key_value]
+    for hop in range(7):
+        ring.append(lax.ppermute(ring[-1], "ep", [(dev, (dev + 1) % 8) for dev in range(8)]))
+    piece_rows = jnp.roll(
+        jnp.concatenate(ring[::-1], axis=0), (lax.axis_index("ep") + 1) * ring[0].shape[0], axis=0
+    )
     piece_count = piece_rows.shape[0]
     length = span_length(piece_count)
     spans = piece_rows.reshape(piece_count // length, length, kv_heads, 2, head_size)

time: 442 us -> 415 us (0.939)
  blocking collectives: 124 us -> 55.6 us
  waiting for transfers between devices: 212 us -> 240 us
  local copies, waits for them, and re-layouts: 33 us -> 44.3 us
    all_gather x1 -> x0, blocking collectives: 68.2 us -> none  [attend(): piece_rows = lax.all_gather(key_value, 'ep', axis=0, tiled=True)]
    ppermute x0 -> x7, waiting for transfers between devices: none -> 46 us  [attend(): lax.ppermute(ring[-1], 'ep', [(dev, (dev + 1) % 8) for dev in range(8)])]
    unnamed x5, waiting for transfers between devices: 147 us -> 106 us
    all_to_all x1, waiting for transfers between devices: 0.01 us -> 31.2 us  [experts_half(): lax.all_to_all(outgoing, 'ep', split_axis=1, concat_axis=0, tiled=True)]
    unnamed x37 -> x52, local copies, waits for them, and re-layouts: 16.9 us -> 26.5 us
    all_gather x1, waiting for transfers between devices: 8.37 us -> 0.01 us  [experts_half(): lax.all_gather(normed.reshape(1, 1, 1, tok_rows, model_width), 'tp', axis...]
  transfers between devices with their start and end apart: 5 -> 12, of which waited for: 3 -> 10; matrix products, arithmetic and copies ran while one was open for 16% -> 20% of each run, Pallas kernels for 0% -> 0%
where the time goes in v1:
time: 415 us; the launch traced here: 414 us
  waiting for transfers between devices  240 us (58%)
  blocking collectives  55.6 us (13%)
  local copies, waits for them, and re-layouts  44.3 us (11%)
  matrix products  26.6 us (6%)
  other arithmetic  26.2 us (6%)
  between operations  14.2 us (3%)
  starting transfers between devices  7.19 us (2%)
    unnamed x5, waiting for transfers between devices  106 us
    all_gather x1, waiting for transfers between devices, experts_half(): lax.all_gather(landed.reshape(local_experts, ep_size, 1, capacity, model_...  56.7 us
    all_to_all x1, blocking collectives, experts_half(): landed = lax.all_to_all(send, 'ep', split_axis=0, concat_axis=1, tiled=True)  55.6 us
    ppermute x7, waiting for transfers between devices, attend(): lax.ppermute(ring[-1], 'ep', [(dev, (dev + 1) % 8) for dev in range(8)])  46 us
    all_to_all x1, waiting for transfers between devices, experts_half(): lax.all_to_all(outgoing, 'ep', split_axis=1, concat_axis=0, tiled=True)  31.2 us
    unnamed x52, local copies, waits for them, and re-layouts  26.5 us
    unnamed x1, other arithmetic  13.2 us
  transfers between devices with their start and end apart: 12, of which 10 were waited for; matrix products, arithmetic and copies ran while one was open for 20% of the time, Pallas kernels for 0%

profile of v1, /device:TPU:0, one launch (start us, length us, event | category | flops | bytes accessed | tf_op | source)
XLA Modules:
  0.0 414.1 jit_solution(17729098434502324406)
XLA Ops:
  9.5 1.4 scatter_custom_fusion
  13.5 3.3 gather_fusion
  16.8 55.6 %all_to_all.8 = bf16[8,64,2048]{2,1,0:T(8,128)(2,1)} all-to-all(bf16[8,64,2048]{2,1,0:T(8,128)(2,1)} %bitcast.110), channel_id=1, replica_groups=mesh['ep'=8,'tp'=4] {'ep'}, dimensions={0} | all-to-all | bytes 4194304 | tf_op jit(solution)/shard_map/all_to_all | solution.py:177
  73.3 56.7 %all-gather.5.cloned.1.call-done = bf16[8,256,2048]{2,1,0:T(8,128)(2,1)} async-done(((bf16[8,64,2048]{2,1,0:T(8,128)(2,1)}), bf16[8,256,2048]{2,1,0:T(8,128)(2,1)}) %all-gather.5.cloned.1.call-update) | async-done | bytes 8388624 | tf_op jit(solution)/shard_map/all_gather | solution.py:179
  129.9 6.0 %fusion.21 = f32[2048,256]{1,0:T(8,128)S(1)} fusion(bf16[2048,2048]{1,0:T(8,128)(2,1)} %bitcast.127, bf16[1,2048,256]{2,1,0:T(8,128)(2,1)S(1)} %copy-done.11), kind=kOutput, calls=%fused_computation.28 | convolution fusion | flops 2147483648 | bytes 11534336 | tf_op jit(solution)/shard_map/lrd,ldf->lrf/dot_general | solution.py:133
  136.0 2.8 fusion.4
  138.7 5.6 %convert_bitcast_fusion = bf16[1,8,4,64,2048]{4,3,2,1,0:T(8,128)(2,1)} fusion(bf16[8,4,64,256]{3,2,1,0:T(8,128)(2,1)S(1)} %bitcast.113, bf16[1,256,2048]{2,1,0:T(8,128)(2,1)S(1)} %copy-done), kind=kOutput, calls=%fused_computation.3 | convolution fusion | flops 2151677952 | bytes 10485760 | tf_op jit(solution)/shard_map/lrf,lfd->lrd/dot_general | solution.py:136
  145.6 1.5 collective-permute-start
  147.3 5.3 %collective-permute-done = bf16[256,128]{0,1:T(8,128)(2,1)S(1)} collective-permute-done((bf16[256,128]{0,1:T(8,128)(2,1)S(1)}, bf16[256,128]{0,1:T(8,128)(2,1)S(1)}, u32[]{:S(2)}, u32[]{:S(2)}) %collective-permute-start) | collective-permute-done | bytes 65568 | tf_op jit(solution)/shard_map/ppermute | solution.py:92
  152.8 6.8 %collective-permute-done.1 = bf16[256,128]{0,1:T(8,128)(2,1)S(1)} collective-permute-done((bf16[256,128]{0,1:T(8,128)(2,1)S(1)}, bf16[256,128]{0,1:T(8,128)(2,1)S(1)}, u32[]{:S(2)}, u32[]{:S(2)}) %collective-permute-start.1) | collective-permute-done | bytes 65568 | tf_op jit(solution)/shard_map/ppermute | solution.py:92
  159.7 6.8 %collective-permute-done.2 = bf16[256,128]{0,1:T(8,128)(2,1)S(1)} collective-permute-done((bf16[256,128]{0,1:T(8,128)(2,1)S(1)}, bf16[256,128]{0,1:T(8,128)(2,1)S(1)}, u32[]{:S(2)}, u32[]{:S(2)}) %collective-permute-start.2) | collective-permute-done | bytes 65568 | tf_op jit(solution)/shard_map/ppermute | solution.py:92
  166.7 6.8 %collective-permute-done.3 = bf16[256,128]{0,1:T(8,128)(2,1)S(1)} collective-permute-done((bf16[256,128]{0,1:T(8,128)(2,1)S(1)}, bf16[256,128]{0,1:T(8,128)(2,1)S(1)}, u32[]{:S(2)}, u32[]{:S(2)}) %collective-permute-start.3) | collective-permute-done | bytes 65568 | tf_op jit(solution)/shard_map/ppermute | solution.py:92
  173.5 7.1 %collective-permute-done.4 = bf16[256,128]{0,1:T(8,128)(2,1)S(1)} collective-permute-done((bf16[256,128]{0,1:T(8,128)(2,1)S(1)}, bf16[256,128]{0,1:T(8,128)(2,1)S(1)}, u32[]{:S(2)}, u32[]{:S(2)}) %collective-permute-start.4) | collective-permute-done | bytes 65568 | tf_op jit(solution)/shard_map/ppermute | solution.py:92
  181.5 6.1 %collective-permute-done.5 = bf16[256,128]{0,1:T(8,128)(2,1)S(1)} collective-permute-done((bf16[256,128]{0,1:T(8,128)(2,1)S(1)}, bf16[256,128]{0,1:T(8,128)(2,1)S(1)}, u32[]{:S(2)}, u32[]{:S(2)}) %collective-permute-start.5) | collective-permute-done | bytes 65568 | tf_op jit(solution)/shard_map/ppermute | solution.py:92
  187.7 7.0 %collective-permute-done.6 = bf16[256,128]{0,1:T(8,128)(2,1)S(1)} collective-permute-done((bf16[256,128]{0,1:T(8,128)(2,1)S(1)}, bf16[256,128]{0,1:T(8,128)(2,1)S(1)}, u32[]{:S(2)}, u32[]{:S(2)}) %collective-permute-start.6) | collective-permute-done | bytes 65568 | tf_op jit(solution)/shard_map/ppermute | solution.py:92
  195.3 3.6 fusion.56
  198.9 5.7 %convolution_convert_fusion = bf16[512,2048]{1,0:T(8,128)(2,1)} fusion(bf16[256,2048]{1,0:T(8,128)(2,1)} %param.29, bf16[512,2048]{1,0:T(8,128)(2,1)S(1)} %copy-done.10, bf16[2048,256]{1,0:T(8,128)(2,1)} %param.28, f32[512,256]{1,0:T(8,128)} %fusion.56), kind=kOutput, calls=%fused_computation.9 | convolution fusion | flops 1075576832 | bytes 6815744 | tf_op jit(solution)/shard_map/dot_general | solution.py:143
  204.6 105.4 %all-reduce.4.cloned.1.call-done = bf16[1,8,4,64,2048]{4,3,2,1,0:T(8,128)(2,1)} async-done(((bf16[1,8,4,64,2048]{4,3,2,1,0:T(8,128)(2,1)}), bf16[1,8,4,64,2048]{4,3,2,1,0:T(8,128)(2,1)}) %all-reduce.4.cloned.1.call-update) | async-done | bytes 8388624
  310.0 2.5 constant_dynamic-slice_fusion.2
  312.5 5.2 %copy.56 = bf16[1,512,2048]{2,0,1:T(2,128)(2,1)} copy(bf16[1,512,2048]{2,1,0:T(8,128)(2,1)S(1)} %bitcast.111) | data formatting | bytes 4194304 | tf_op jit(solution)/shard_map/reshape | solution.py:210
  318.2 13.2 %reduce.9 = bf16[512,2048]{1,0:T(8,128)(2,1)S(1)} reduce(bf16[512,1,2048]{2,1,0:T(2,128)(2,1)} %bitcast.108, bf16[]{:T(256)} %broadcast.383), dimensions={1}, to_apply=%bitcast.106.reduce_sub_computation | reduce | bytes 4194306
  331.4 3.8 reshape.653
  335.2 5.5 %all-to-all-start.1 = ((bf16[8,2,65536]{2,1,0:T(2,128)(2,1)}), bf16[8,2,65536]{2,1,0:T(2,128)(2,1)S(1)}, u32[]{:S(2)}, u32[]{:S(2)}) async-start(bf16[8,2,65536]{2,1,0:T(2,128)(2,1)} %reshape.653), calls=%async_computation.1 | async-start | bytes 4194304 | tf_op jit(solution)/shard_map/all_to_all | solution.py:213
  352.9 1.9 fusion
  354.8 1.7 fusion.12
  357.4 31.2 %all-to-all-done.1 = bf16[8,2,65536]{2,1,0:T(2,128)(2,1)S(1)} async-done(((bf16[8,2,65536]{2,1,0:T(2,128)(2,1)}), bf16[8,2,65536]{2,1,0:T(2,128)(2,1)S(1)}, u32[]{:S(2)}, u32[]{:S(2)}) %all-to-all-start.1) | async-done | bytes 2097184 | tf_op jit(solution)/shard_map/all_to_all | solution.py:213
  388.6 4.4 %reshape.654 = bf16[512,1,2048]{2,1,0:T(2,128)(2,1)} reshape(bf16[8,2,65536]{2,1,0:T(2,128)(2,1)S(1)} %all-to-all-done.1) | data formatting | bytes 4194304
  393.0 3.5 copy.55
  396.5 2.3 gather_fusion.1
  398.8 2.5 reshape.614
  401.3 4.1 multiply_reduce_fusion.1
  405.4 2.3 fusion.18
  (116 shorter events, 22.4 us)
Async XLA Ops:
  7.2 131.6 %copy-start = (bf16[1,256,2048]{2,1,0:T(8,128)(2,1)S(1)}, bf16[1,256,2048]{2,1,0:T(8,128)(2,1)}, u32[]{:S(2)}) copy-start(bf16[1,256,2048]{2,1,0:T(8,128)(2,1)} %param.26) | copy-start | bytes 3145732
  7.2 122.7 %all-gather.5.cloned.1.call-start = ((), (), s32[]{:S(2)}) async-start(), calls=%async_computation.4 | async-start | bytes 10485760 | tf_op jit(solution)/shard_map/all_gather | solution.py:179
  13.4 3.4 copy-start.2
  72.4 57.5 %copy-start.11 = (bf16[1,2048,256]{2,1,0:T(8,128)(2,1)S(1)}, bf16[1,2048,256]{2,1,0:T(8,128)(2,1)}, u32[]{:S(2)}) copy-start(bf16[1,2048,256]{2,1,0:T(8,128)(2,1)} %param.24) | copy-start | bytes 3145732
  72.5 122.8 %all-gather.7.cloned.1.call-start = ((), (), s32[]{:S(2)}) async-start(), calls=%async_computation.5 | async-start | bytes 2621440 | tf_op jit(solution)/shard_map/all_gather | solution.py:185
  73.2 236.8 %all-reduce.4.cloned.1.call-start = ((), (), s32[]{:S(2)}) async-start(), calls=%async_computation.6 | async-start | bytes 16777216
  129.9 6.0 %copy-start.9 = (bf16[8,256,2048]{2,1,0:T(8,128)(2,1)S(1)}, bf16[8,256,2048]{2,1,0:T(8,128)(2,1)}, u32[]{:S(2)}) copy-start(bf16[8,256,2048]{2,1,0:T(8,128)(2,1)} %all-gather.5.cloned.1.call-done) | copy-start | bytes 25165828
  129.9 6.0 %copy-start.12 = (bf16[1,2048,256]{2,1,0:T(8,128)(2,1)S(1)}, bf16[1,2048,256]{2,1,0:T(8,128)(2,1)}, u32[]{:S(2)}) copy-start(bf16[1,2048,256]{2,1,0:T(8,128)(2,1)} %param.25) | copy-start | bytes 3145732
  144.3 0.8 copy-start.3
  144.3 0.8 copy-start.7
  144.3 1.3 copy-start.5
  144.3 2.8 copy-start.4
  144.3 8.3 %copy-start.8 = (f32[64]{0:T(128)S(1)}, f32[64]{0:T(128)}, u32[]{:S(2)}) copy-start(f32[64]{0:T(128)} %param.18) | copy-start | bytes 772
  144.3 22.2 %copy-start.6 = (f32[512,2]{0,1:T(2,128)S(1)}, f32[512,2]{0,1:T(2,128)}, u32[]{:S(2)}) copy-start(f32[512,2]{0,1:T(2,128)} %param.23) | copy-start | bytes 12292
  144.3 36.6 %copy-start.13 = (u32[32]{0:T(128)S(1)}, u32[32]{0:T(128)}, u32[]{:S(2)}) copy-start(u32[32]{0:T(128)} %constant.148) | copy-start | bytes 388
  144.4 261.0 %reduce-scatter.5.cloned.1.call-start = ((), (), s32[]{:S(2)}) async-start(), calls=%async_computation.3 | async-start | bytes 2621440 | tf_op jit(solution)/shard_map/reduce_scatter | solution.py:203
  145.6 7.0 %collective-permute-start = (bf16[256,128]{0,1:T(8,128)(2,1)S(1)}, bf16[256,128]{0,1:T(8,128)(2,1)S(1)}, u32[]{:S(2)}, u32[]{:S(2)}) collective-permute-start(bf16[256,128]{0,1:T(8,128)(2,1)S(1)} %bitcast.117), channel_id=1, source_target_pairs={{0,4},{4,8},{8,12},{12,16},{16,20},{20,24},{24,28},{28,0},{1,5},{5... | collective-permute-start | bytes 196616 | tf_op jit(solution)/shard_map/ppermute | solution.py:92
  152.6 7.0 %collective-permute-start.1 = (bf16[256,128]{0,1:T(8,128)(2,1)S(1)}, bf16[256,128]{0,1:T(8,128)(2,1)S(1)}, u32[]{:S(2)}, u32[]{:S(2)}) collective-permute-start(bf16[256,128]{0,1:T(8,128)(2,1)S(1)} %collective-permute-done), channel_id=1, source_target_pairs={{0,4},{4,8},{8,12},{12,16},{16,20},{20,24},{24,28},{28,0},{1,5},{5... | collective-permute-start | bytes 196616 | tf_op jit(solution)/shard_map/ppermute | solution.py:92
  159.6 7.0 %collective-permute-start.2 = (bf16[256,128]{0,1:T(8,128)(2,1)S(1)}, bf16[256,128]{0,1:T(8,128)(2,1)S(1)}, u32[]{:S(2)}, u32[]{:S(2)}) collective-permute-start(bf16[256,128]{0,1:T(8,128)(2,1)S(1)} %collective-permute-done.1), channel_id=1, source_target_pairs={{0,4},{4,8},{8,12},{12,16},{16,20},{20,24},{24,28},{28,0},{1,5},{5... | collective-permute-start | bytes 196616 | tf_op jit(solution)/shard_map/ppermute | solution.py:92
  166.5 7.0 %collective-permute-start.3 = (bf16[256,128]{0,1:T(8,128)(2,1)S(1)}, bf16[256,128]{0,1:T(8,128)(2,1)S(1)}, u32[]{:S(2)}, u32[]{:S(2)}) collective-permute-start(bf16[256,128]{0,1:T(8,128)(2,1)S(1)} %collective-permute-done.2), channel_id=1, source_target_pairs={{0,4},{4,8},{8,12},{12,16},{16,20},{20,24},{24,28},{28,0},{1,5},{5... | collective-permute-start | bytes 196616 | tf_op jit(solution)/shard_map/ppermute | solution.py:92
  173.5 7.2 %collective-permute-start.4 = (bf16[256,128]{0,1:T(8,128)(2,1)S(1)}, bf16[256,128]{0,1:T(8,128)(2,1)S(1)}, u32[]{:S(2)}, u32[]{:S(2)}) collective-permute-start(bf16[256,128]{0,1:T(8,128)(2,1)S(1)} %collective-permute-done.3), channel_id=1, source_target_pairs={{0,4},{4,8},{8,12},{12,16},{16,20},{20,24},{24,28},{28,0},{1,5},{5... | collective-permute-start | bytes 196616 | tf_op jit(solution)/shard_map/ppermute | solution.py:92
  180.6 7.0 %collective-permute-start.5 = (bf16[256,128]{0,1:T(8,128)(2,1)S(1)}, bf16[256,128]{0,1:T(8,128)(2,1)S(1)}, u32[]{:S(2)}, u32[]{:S(2)}) collective-permute-start(bf16[256,128]{0,1:T(8,128)(2,1)S(1)} %collective-permute-done.4), channel_id=1, source_target_pairs={{0,4},{4,8},{8,12},{12,16},{16,20},{20,24},{24,28},{28,0},{1,5},{5... | collective-permute-start | bytes 196616 | tf_op jit(solution)/shard_map/ppermute | solution.py:92
  187.7 7.0 %collective-permute-start.6 = (bf16[256,128]{0,1:T(8,128)(2,1)S(1)}, bf16[256,128]{0,1:T(8,128)(2,1)S(1)}, u32[]{:S(2)}, u32[]{:S(2)}) collective-permute-start(bf16[256,128]{0,1:T(8,128)(2,1)S(1)} %collective-permute-done.5), channel_id=1, source_target_pairs={{0,4},{4,8},{8,12},{12,16},{16,20},{20,24},{24,28},{28,0},{1,5},{5... | collective-permute-start | bytes 196616 | tf_op jit(solution)/shard_map/ppermute | solution.py:92
  195.3 3.6 copy-start.10
  335.2 53.4 %all-to-all-start.1 = ((bf16[8,2,65536]{2,1,0:T(2,128)(2,1)}), bf16[8,2,65536]{2,1,0:T(2,128)(2,1)S(1)}, u32[]{:S(2)}, u32[]{:S(2)}) async-start(bf16[8,2,65536]{2,1,0:T(2,128)(2,1)} %reshape.653), calls=%async_computation.1 | async-start | bytes 4194304 | tf_op jit(solution)/shard_map/all_to_all | solution.py:213
  398.8 8.8 %copy-start.1 = (bf16[1,256,2048]{2,1,0:T(8,128)(2,1)S(1)}, bf16[1,256,2048]{2,1,0:T(8,128)(2,1)}, u32[]{:S(2)}) copy-start(bf16[1,256,2048]{2,1,0:T(8,128)(2,1)} %param.26) | copy-start | bytes 3145732
Sparse Core Ops, SparseCore 0:
  72.6 57.2 all-gather.4
  132.0 22.5 all-gather.6
  157.1 152.8 all-reduce.3
  312.4 31.3 reduce-scatter.4
